TPU v7x, 32 devices: a whole 2x2x4 slice. The times are simulated.
32 devices in a mesh: rep: 2 (over x), fs: 8 (over z, y), tp: 2 (over core).
Axes of the slice: x: 2, y: 2, z: 4, core: 2. Of those that a mesh axis runs over, the one named last changes fastest.
Arguments:
- inputs: bfloat16 [8192, 1024], P(('rep', 'fs', 'tp')), may hold values from -6 to 6
- up_proj: bfloat16 [1024, 4096], P('fs', 'tp'), may hold values from -0.1875 to 0.1875
- down_proj: bfloat16 [4096, 1024], P('tp', 'fs'), may hold values from -0.09375 to 0.09375
- out_cotangent: bfloat16 [8192, 1024], P(('rep', 'fs', 'tp')), may hold values from -6 to 6
Outputs:
- grad_inputs: bfloat16 [8192, 1024], P(('rep', 'fs', 'tp'))
- grad_up: float32 [1024, 4096], P('fs', 'tp')
- grad_down: float32 [4096, 1024], P('tp', 'fs')
- energy_up: float32 [1024], P('fs')
- energy_down: float32 [4096], P('tp')
All inputs are finite; a program needn't handle non-finite values.
Results may differ from a plain program's by a relative error of at most 0.001.
Values may be sent and summed in bfloat16 or wider, within the bound.
A program may use at most 128 MiB of HBM per device.

v0:
```python
import jax
import jax.numpy as jnp
from jax import lax
from jax.sharding import PartitionSpec as P

D = 1024
FF = 4096


def taken_in(shard, axis, dim, absorb, state):
    everything = jax.tree.map(lambda a: lax.all_gather(a, axis, axis=dim, tiled=True), shard)
    return absorb(state, everything, jnp.int32(0))


def summed_rows(product, span, axis):
    whole = product(jnp.int32(0), span * lax.axis_size(axis))
    return lax.psum_scatter(whole, axis, scatter_dimension=0, tiled=True)


def contract(left, right, left_dim, right_dim):
    return lax.dot_general(
        left, right, (((left_dim,), (right_dim,)), ((), ())), preferred_element_type=jnp.float32
    )


def body(inputs, up_proj, down_proj, out_cotangent):
    factor = float(
        inputs.shape[0] * lax.axis_size("rep") * lax.axis_size("fs") * lax.axis_size("tp")
    ) ** (-0.5)
    all_inputs, all_cotangent = (
        lax.all_gather(inputs, "tp", axis=0, tiled=True),
        lax.all_gather(out_cotangent, "tp", axis=0, tiled=True),
    )
    hidden_cols = up_proj.shape[1]
    group_rows = all_inputs.shape[0]
    whole_up = lax.all_gather(up_proj, "fs", axis=0, tiled=True)
    pre = jnp.dot(all_inputs, whole_up, preferred_element_type=jnp.float32)
    active = jnp.square(jax.nn.relu(pre)).astype(jnp.bfloat16)

    def add_cols(total, piece, start):
        columns = lax.dynamic_slice_in_dim(all_cotangent, start, piece.shape[1], 1)
        return total + contract(columns, piece, 1, 1)

    back = taken_in(down_proj, "fs", 1, add_cols, jnp.zeros((group_rows, hidden_cols), jnp.float32))
    grad_pre = (2.0 * jax.nn.relu(pre) * back).astype(jnp.bfloat16)

    def input_part(start, count):
        rows = lax.dynamic_slice_in_dim(grad_pre, start, count, 0)
        return contract(rows, whole_up, 1, 1)

    grad_inputs = summed_rows(input_part, inputs.shape[0], "tp")
    grad_inputs = grad_inputs.astype(jnp.bfloat16)
    shard_rows = up_proj.shape[0]

    def up_part(start, count):
        columns = lax.dynamic_slice_in_dim(all_inputs, start, count, 1)
        return contract(columns, grad_pre, 0, 0) * factor

    def down_part(start, count):
        columns = lax.dynamic_slice_in_dim(all_cotangent, start, count, 1)
        return contract(columns, active, 0, 0) * factor

    def joint_part(start, count):
        return jnp.concatenate([up_part(start, count), down_part(start, count)], axis=1)

    joint_local = summed_rows(joint_part, shard_rows, "fs")
    joint_sum = lax.psum(joint_local, "rep")
    grad_up = joint_sum[:, :hidden_cols]
    down_flip = joint_sum[:, hidden_cols:]
    grad_down = jnp.transpose(down_flip)
    energy_up = lax.psum(jnp.sum(grad_up * grad_up, axis=1), "tp") / FF
    energy_down = lax.psum(jnp.sum(grad_down * grad_down, axis=1), "fs") / D
    return (grad_inputs, grad_up, grad_down, energy_up, energy_down)


def solution(mesh):
    return jax.shard_map(
        body,
        mesh=mesh,
        in_specs=(
            P(("rep", "fs", "tp"), None),
            P("fs", "tp"),
            P("tp", "fs"),
            P(("rep", "fs", "tp"), None),
        ),
        out_specs=(P(("rep", "fs", "tp"), None), P("fs", "tp"), P("tp", "fs"), P("fs"), P("tp")),
        check_vma=False,
    )
```

profile of v0, /device:TPU:0, one launch (start us, length us, event | category | flops | bytes accessed | tf_op | source)
XLA Modules:
  0.0 594.2 jit_solution(6875754057752719887)
XLA Ops:
  7.2 0.0 all-gather.5.cloned.1.call-start
  7.2 0.7 all-gather.5.cloned.1.call-update
  7.9 0.0 all-gather.7.cloned.1.call-start
  7.9 0.7 all-gather.7.cloned.1.call-update
  8.6 0.0 all-gather.9.cloned.1.call-start
  8.7 0.7 all-gather.9.cloned.1.call-update
  9.4 0.0 all-gather.11.cloned.1.call-start
  9.4 0.5 all-gather.11.cloned.1.call-update
  10.0 0.0 reduce-scatter.5.cloned.1.call-start
  10.0 11.3 %all-gather.5.cloned.1.call-done = bf16[512,1024]{1,0:T(8,128)(2,1)} async-done(((bf16[256,1024]{1,0:T(8,128)(2,1)}), bf16[512,1024]{1,0:T(8,128)(2,1)}) %all-gather.5.cloned.1.call-update) | async-done | bytes 1048592 | tf_op jit(solution)/shard_map/all_gather | solution.py:31
  21.3 76.1 %all-gather.7.cloned.1.call-done = bf16[1024,2048]{1,0:T(8,128)(2,1)} async-done(((bf16[128,2048]{1,0:T(8,128)(2,1)}), bf16[1024,2048]{1,0:T(8,128)(2,1)}) %all-gather.7.cloned.1.call-update) | async-done | bytes 4194320 | tf_op jit(solution)/shard_map/all_gather | solution.py:36
  97.4 6.8 %fusion.2 = f32[512,2048]{1,0:T(8,128)} fusion(bf16[512,1024]{1,0:T(8,128)(2,1)} %all-gather.5.cloned.1.call-done, bf16[1024,2048]{1,0:T(8,128)(2,1)} %all-gather.7.cloned.1.call-done), kind=kOutput, calls=%fused_computation.12 | convolution fusion | flops 2147483648 | bytes 9437184 | tf_op jit(solution)/shard_map/dot_general | solution.py:37
  104.2 2.4 all-gather.9.cloned.1.call-done
  106.6 0.0 copy-start.1
  106.6 8.2 %multiply_bitcast_fusion = f32[1024,2048]{0,1:T(8,128)} fusion(bf16[512,1024]{1,0:T(8,128)(2,1)} %all-gather.9.cloned.1.call-done, f32[512,2048]{1,0:T(8,128)} %fusion.2), kind=kOutput, calls=%fused_computation.1 | convolution fusion | flops 2152726528 | bytes 13631488 | tf_op jit(solution)/shard_map/dot_general | solution.py:21
  114.8 0.0 copy-start.2
  114.8 69.5 %all-gather.11.cloned.1.call-done = bf16[2048,1024]{1,0:T(8,128)(2,1)} async-done(((bf16[2048,128]{1,0:T(8,128)(2,1)}), bf16[2048,1024]{1,0:T(8,128)(2,1)}) %all-gather.11.cloned.1.call-update) | async-done | bytes 4194320 | tf_op jit(solution)/shard_map/all_gather | solution.py:11
  184.3 0.0 copy-done.1
  184.3 5.9 multiply_convert_fusion.1
  190.2 0.0 copy-done.2
  190.2 0.0 copy-start.3
  190.2 0.0 copy-start
  190.2 2.4 multiply_bitcast_fusion.1
  192.6 0.0 copy-done.3
  192.6 1.7 copy-done
  194.3 6.4 %pad_maximum_fusion = f32[1024,4096]{0,1:T(8,128)} fusion(f32[1024,2048]{0,1:T(8,128)S(1)} %copy-done, f32[1024,2048]{0,1:T(8,128)S(1)} %multiply_bitcast_fusion.1), kind=kLoop, calls=%fused_computation | loop fusion | flops 4194304 | bytes 33554432 | tf_op jit(solution)/shard_map/concatenate | solution.py:64
  200.7 0.0 copy-start.4
  200.7 0.0 reduce-scatter.5.cloned.1.call-update
  200.8 0.0 reduce-scatter.3.cloned.1.call-start
  200.8 1.5 copy-done.4
  202.3 5.9 fusion.3
  208.2 0.0 reduce-scatter.3.cloned.1.call-update
  208.3 0.0 all-reduce.2.cloned.1.call-start
  208.3 271.0 %reduce-scatter.5.cloned.1.call-done = f32[128,4096]{0,1:T(8,128)} async-done(((f32[1024,4096]{0,1:T(8,128)}), f32[128,4096]{0,1:T(8,128)}) %reduce-scatter.5.cloned.1.call-update) | async-done | bytes 2097168 | tf_op jit(solution)/shard_map/reduce_scatter | solution.py:17
  479.3 0.0 all-reduce.2.cloned.1.call-update
  479.4 11.0 %reduce-scatter.3.cloned.1.call-done = f32[256,1024]{1,0:T(8,128)} async-done(((f32[512,1024]{1,0:T(8,128)}), f32[256,1024]{1,0:T(8,128)}) %reduce-scatter.3.cloned.1.call-update) | async-done | bytes 1048592 | tf_op jit(solution)/shard_map/reduce_scatter | solution.py:17
  490.3 2.1 convert_element_type.10
  492.4 64.5 %all-reduce.2.cloned.1.call-done = f32[128,4096]{0,1:T(8,128)} async-done(((f32[128,4096]{0,1:T(8,128)}), f32[128,4096]{0,1:T(8,128)}) %all-reduce.2.cloned.1.call-update) | async-done | bytes 2097168 | tf_op jit(solution)/shard_map/psum | solution.py:67
  556.9 2.4 multiply_reduce_fusion
  559.3 21.7 %psum.23 = f32[2048]{0:T(1024)S(1)} all-reduce(f32[2048]{0:T(1024)S(1)} %get-tuple-element.10), channel_id=1, replica_groups=mesh['rep'=2,'fs'=8,'tp'=2] {'fs'}, use_global_device_ids=true, to_apply=%region_6.7 | all-reduce | flops 2048 | bytes 16384 | tf_op jit(solution)/shard_map/psum | solution.py:72
  581.0 0.6 broadcast_multiply_fusion
  581.6 1.5 multiply_reduce_fusion.1
  583.1 2.5 psum.22
  585.6 0.5 broadcast_multiply_fusion.1
  586.1 1.3 copy.9
Async XLA Ops:
  7.2 14.1 %all-gather.5.cloned.1.call-start = ((), (), s32[]{:S(2)}) async-start(), calls=%async_computation.2 | async-start | bytes 1572864 | tf_op jit(solution)/shard_map/all_gather | solution.py:31
  7.9 89.5 %all-gather.7.cloned.1.call-start = ((), (), s32[]{:S(2)}) async-start(), calls=%async_computation.3 | async-start | bytes 4718592 | tf_op jit(solution)/shard_map/all_gather | solution.py:36
  8.6 97.9 %all-gather.9.cloned.1.call-start = ((), (), s32[]{:S(2)}) async-start(), calls=%async_computation.4 | async-start | bytes 1572864 | tf_op jit(solution)/shard_map/all_gather | solution.py:32
  9.4 174.9 %all-gather.11.cloned.1.call-start = ((), (), s32[]{:S(2)}) async-start(), calls=%async_computation.5 | async-start | bytes 4718592 | tf_op jit(solution)/shard_map/all_gather | solution.py:11
  10.0 469.4 %reduce-scatter.5.cloned.1.call-start = ((), (), s32[]{:S(2)}) async-start(), calls=%async_computation.7 | async-start | bytes 18874368 | tf_op jit(solution)/shard_map/reduce_scatter | solution.py:17
  106.6 77.7 %copy-start.1 = (bf16[512,1024]{1,0:T(8,128)(2,1)S(1)}, bf16[512,1024]{1,0:T(8,128)(2,1)}, u32[]{:S(2)}) copy-start(bf16[512,1024]{1,0:T(8,128)(2,1)} %all-gather.9.cloned.1.call-done) | copy-start | bytes 3145732
  114.8 75.4 %copy-start.2 = (bf16[512,1024]{1,0:T(8,128)(2,1)S(1)}, bf16[512,1024]{1,0:T(8,128)(2,1)}, u32[]{:S(2)}) copy-start(bf16[512,1024]{1,0:T(8,128)(2,1)} %all-gather.5.cloned.1.call-done) | copy-start | bytes 3145732
  190.2 2.4 copy-start.3
  190.2 4.1 copy-start
  200.7 1.6 copy-start.4
  200.8 289.6 %reduce-scatter.3.cloned.1.call-start = ((), (), s32[]{:S(2)}) async-start(), calls=%async_computation.6 | async-start | bytes 3145728 | tf_op jit(solution)/shard_map/reduce_scatter | solution.py:17
  208.3 348.7 %all-reduce.2.cloned.1.call-start = ((), (), s32[]{:S(2)}) async-start(), calls=%async_computation.8 | async-start | bytes 4194304 | tf_op jit(solution)/shard_map/psum | solution.py:67
Sparse Core Ops, SparseCore 0:
  9.5 11.7 all-gather.4
  23.4 73.9 all-gather.6
  99.0 7.5 all-gather.8
  108.5 75.7 all-gather.10
  200.9 278.4 reduce-scatter.4
  481.4 8.8 reduce-scatter.2
  492.6 64.2 all-reduce.1
where the time goes:
time: 595 us; the launch traced here: 594 us
  waiting for transfers between devices  508 us (85%)
  matrix products  29.2 us (5%)
  blocking collectives  24.1 us (4%)
  between operations  14.2 us (2%)
  other arithmetic  13.5 us (2%)
    reduce_scatter x2, waiting for transfers between devices, summed_rows(): return lax.psum_scatter(whole, axis, scatter_dimension=0, tiled=True)  282 us
    all_gather x1, waiting for transfers between devices, body(): whole_up = lax.all_gather(up_proj, 'fs', axis=0, tiled=True)  76.1 us
    all_gather x1, waiting for transfers between devices, taken_in(): lax.all_gather(a, axis, axis=dim, tiled=True)  69.5 us
    psum x1, waiting for transfers between devices, body(): joint_sum = lax.psum(joint_local, 'rep')  64.5 us
    dot_general x4, matrix products, contract(): lax.dot_general(left, right, (((left_dim,), (right_dim,)), ((), ())), pre...  22.4 us
    psum x1, blocking collectives, body(): energy_down = lax.psum(jnp.sum(grad_down * grad_down, axis=1), 'fs') / D  21.7 us
  transfers between devices with their start and end apart: 7, of which 7 were waited for; matrix products, arithmetic and copies ran while one was open for 4% of the time, Pallas kernels for 0%

commit v1 on v0

--- a/solution.py
+++ b/solution.py
@@ -33,7 +33,21 @@
     )
     hidden_cols = up_proj.shape[1]
     group_rows = all_inputs.shape[0]
-    whole_up = lax.all_gather(up_proj, "fs", axis=0, tiled=True)
+    ways, here, step = (lax.axis_size("fs"), lax.axis_index("fs"), up_proj.shape[0])
+    shape = [n * ways if d == 0 else n for d, n in enumerate(up_proj.shape)]
+    full = lax.dynamic_update_slice_in_dim(
+        jnp.zeros(shape, up_proj.dtype), up_proj, here * step, axis=0
+    )
+    going_up = going_down = up_proj
+    for far in range(1, ways // 2 + 1):
+        going_up = lax.ppermute(going_up, "fs", [(d, (d + 1) % ways) for d in range(ways)])
+        full = lax.dynamic_update_slice_in_dim(full, going_up, (here - far) % ways * step, axis=0)
+        if 2 * far < ways:
+            going_down = lax.ppermute(going_down, "fs", [(d, (d - 1) % ways) for d in range(ways)])
+            full = lax.dynamic_update_slice_in_dim(
+                full, going_down, (here + far) % ways * step, axis=0
+            )
+    whole_up = full
     pre = jnp.dot(all_inputs, whole_up, preferred_element_type=jnp.float32)
     active = jnp.square(jax.nn.relu(pre)).astype(jnp.bfloat16)
 

time: 595 us -> 553 us (0.929)
  waiting for transfers between devices: 508 us -> 440 us
  starting transfers between devices: 0.27 us -> 17.6 us
  local copies, waits for them, and re-layouts: 4.54 us -> 14.2 us
    ppermute x0 -> x7, waiting for transfers between devices: none -> 82.9 us  [the longest x4 82.9 us: body(): lax.ppermute(going_up, 'fs', [(d, (d + 1) % ways) for d in range(ways)])]
    all_gather x1 -> x0, waiting for transfers between devices: 76.1 us -> none  [body(): whole_up = lax.all_gather(up_proj, 'fs', axis=0, tiled=True)]
    all_gather x1, waiting for transfers between devices: 69.5 us -> 7.24 us  [taken_in(): lax.all_gather(a, axis, axis=dim, tiled=True)]
    ppermute x0 -> x7, starting transfers between devices: none -> 17.1 us  [the longest x3 9.23 us: body(): lax.ppermute(going_down, 'fs', [(d, (d - 1) % ways) for d in range(ways)])]
    all_gather x1, waiting for transfers between devices: 11.3 us -> 0.01 us  [body(): lax.all_gather(inputs, 'tp', axis=0, tiled=True)]
    dynamic_update_slice x0 -> x8, local copies, waits for them, and re-layouts: none -> 6.72 us  [the longest x4 3.36 us: body(): lax.dynamic_update_slice_in_dim(full, going_up, (here - far) % ways * ste...]
  transfers between devices with their start and end apart: 7 -> 13, of which waited for: 7 -> 8; matrix products, arithmetic and copies ran while one was open for 4% -> 6% of each run, Pallas kernels for 0% -> 0%
where the time goes in v1:
time: 553 us; the launch traced here: 552 us
  waiting for transfers between devices  440 us (80%)
  matrix products  29.2 us (5%)
  blocking collectives  24.1 us (4%)
  starting transfers between devices  17.6 us (3%)
  local copies, waits for them, and re-layouts  14.2 us (3%)
  between operations  14.2 us (3%)
  other arithmetic  13.5 us (2%)
    reduce_scatter x2, waiting for transfers between devices, summed_rows(): return lax.psum_scatter(whole, axis, scatter_dimension=0, tiled=True)  283 us
    ppermute x4, waiting for transfers between devices, body(): lax.ppermute(going_up, 'fs', [(d, (d + 1) % ways) for d in range(ways)])  82.9 us
    psum x1, waiting for transfers between devices, body(): joint_sum = lax.psum(joint_local, 'rep')  64.3 us
    dot_general x4, matrix products, contract(): lax.dot_general(left, right, (((left_dim,), (right_dim,)), ((), ())), pre...  22.4 us
    psum x1, blocking collectives, body(): energy_down = lax.psum(jnp.sum(grad_down * grad_down, axis=1), 'fs') / D  21.7 us
  transfers between devices with their start and end apart: 13, of which 8 were waited for; matrix products, arithmetic and copies ran while one was open for 6% of the time, Pallas kernels for 0%

profile of v1, /device:TPU:0, one launch (start us, length us, event | category | flops | bytes accessed | tf_op | source)
XLA Modules:
  0.0 552.4 jit_solution(3518960255673162978)
XLA Ops:
  7.2 0.0 copy-start.2
  7.2 0.0 all-gather.4.cloned.1.call-start
  7.2 0.7 all-gather.4.cloned.1.call-update
  7.9 0.0 all-gather.6.cloned.1.call-start
  8.0 0.7 all-gather.6.cloned.1.call-update
  8.7 0.0 all-gather.8.cloned.1.call-start
  8.7 0.7 all-gather.8.cloned.1.call-update
  9.4 0.0 reduce-scatter.5.cloned.1.call-start
  9.4 3.0 collective-permute-start
  12.5 3.1 collective-permute-start.1
  15.6 19.6 %collective-permute-done = bf16[128,2048]{1,0:T(8,128)(2,1)S(1)} collective-permute-done((bf16[128,2048]{1,0:T(8,128)(2,1)}, bf16[128,2048]{1,0:T(8,128)(2,1)S(1)}, u32[]{:S(2)}, u32[]{:S(2)}) %collective-permute-start) | collective-permute-done | bytes 524320 | tf_op jit(solution)/shard_map/ppermute | solution.py:43
  35.2 2.4 collective-permute-start.2
  37.6 0.0 collective-permute-done.1
  37.6 3.0 collective-permute-start.3
  40.6 2.5 broadcast_in_dim.3
  43.1 0.0 copy-done.2
  43.1 0.8 constant_dynamic-update-slice_fusion.7
  44.0 20.8 %collective-permute-done.2 = bf16[128,2048]{1,0:T(8,128)(2,1)S(1)} collective-permute-done((bf16[128,2048]{1,0:T(8,128)(2,1)S(1)}, bf16[128,2048]{1,0:T(8,128)(2,1)S(1)}, u32[]{:S(2)}, u32[]{:S(2)}) %collective-permute-start.2) | collective-permute-done | bytes 524320 | tf_op jit(solution)/shard_map/ppermute | solution.py:43
  64.8 2.5 collective-permute-start.4
  67.3 0.8 constant_dynamic-update-slice_fusion.6
  68.1 0.8 constant_dynamic-update-slice_fusion.5
  68.9 0.0 collective-permute-done.3
  68.9 3.1 collective-permute-start.5
  72.0 0.8 constant_dynamic-update-slice_fusion.4
  72.9 18.5 %collective-permute-done.4 = bf16[128,2048]{1,0:T(8,128)(2,1)S(1)} collective-permute-done((bf16[128,2048]{1,0:T(8,128)(2,1)S(1)}, bf16[128,2048]{1,0:T(8,128)(2,1)S(1)}, u32[]{:S(2)}, u32[]{:S(2)}) %collective-permute-start.4) | collective-permute-done | bytes 524320 | tf_op jit(solution)/shard_map/ppermute | solution.py:43
  91.3 0.0 collective-permute-start.6
  91.3 0.8 constant_dynamic-update-slice_fusion.3
  92.2 0.8 constant_dynamic-update-slice_fusion.2
  93.0 0.0 collective-permute-done.5
  93.0 0.8 constant_dynamic-update-slice_fusion.1
  93.9 24.0 %collective-permute-done.6 = bf16[128,2048]{1,0:T(8,128)(2,1)S(1)} collective-permute-done((bf16[128,2048]{1,0:T(8,128)(2,1)S(1)}, bf16[128,2048]{1,0:T(8,128)(2,1)S(1)}, u32[]{:S(2)}, u32[]{:S(2)}) %collective-permute-start.6) | collective-permute-done | bytes 524320 | tf_op jit(solution)/shard_map/ppermute | solution.py:43
  117.9 0.8 constant_dynamic-update-slice_fusion
  118.7 0.0 all-gather.4.cloned.1.call-done
  118.7 6.8 %fusion.3 = f32[2048,512]{1,0:T(8,128)} fusion(bf16[1024,2048]{1,0:T(8,128)(2,1)} %constant_dynamic-update-slice_fusion, bf16[512,1024]{1,0:T(8,128)(2,1)} %all-gather.4.cloned.1.call-done), kind=kOutput, calls=%fused_computation.21 | convolution fusion | flops 2147483648 | bytes 9437184 | tf_op jit(solution)/shard_map/dot_general | solution.py:51
  125.5 0.0 all-gather.6.cloned.1.call-done
  125.5 0.0 copy-start.1
  125.5 8.1 %multiply_bitcast_fusion = f32[1024,2048]{0,1:T(8,128)} fusion(bf16[512,1024]{1,0:T(8,128)(2,1)} %all-gather.6.cloned.1.call-done, f32[2048,512]{1,0:T(8,128)} %fusion.3), kind=kOutput, calls=%fused_computation.1 | convolution fusion | flops 2152726528 | bytes 13631488 | tf_op jit(solution)/shard_map/dot_general | solution.py:21
  133.7 7.2 %all-gather.8.cloned.1.call-done = bf16[2048,1024]{1,0:T(8,128)(2,1)} async-done(((bf16[2048,128]{1,0:T(8,128)(2,1)}), bf16[2048,1024]{1,0:T(8,128)(2,1)}) %all-gather.8.cloned.1.call-update) | async-done | bytes 4194320 | tf_op jit(solution)/shard_map/all_gather | solution.py:11
  140.9 0.0 copy-done.1
  140.9 6.0 %fusion = bf16[512,2048]{0,1:T(8,128)(2,1)S(1)} fusion(f32[2048,512]{1,0:T(8,128)} %fusion.3, bf16[512,1024]{1,0:T(8,128)(2,1)S(1)} %copy-done.1, bf16[2048,1024]{1,0:T(8,128)(2,1)} %all-gather.8.cloned.1.call-done), kind=kOutput, calls=%fused_computation.4 | convolution fusion | flops 2151677952 | bytes 11534336 | tf_op jit(solution)/shard_map/dot_general | solution.py:21
  146.9 0.0 copy-start.4
  146.9 1.3 copy-done.4
  148.2 0.0 copy-done.3
  148.2 2.4 multiply_bitcast_fusion.1
  150.6 1.0 copy-done
  151.6 6.4 %pad_maximum_fusion = f32[1024,4096]{0,1:T(8,128)} fusion(f32[1024,2048]{0,1:T(8,128)S(1)} %copy-done, f32[1024,2048]{0,1:T(8,128)S(1)} %multiply_bitcast_fusion.1), kind=kLoop, calls=%fused_computation | loop fusion | flops 4194304 | bytes 33554432 | tf_op jit(solution)/shard_map/concatenate | solution.py:78
  158.0 0.0 reduce-scatter.5.cloned.1.call-update
  158.0 0.2 reduce-scatter.3.cloned.1.call-start
  158.2 1.3 copy-done.5
  159.6 5.9 %fusion.4 = f32[512,1024]{1,0:T(8,128)} fusion(bf16[512,2048]{0,1:T(8,128)(2,1)S(1)} %copy-done.5, bf16[1024,2048]{1,0:T(8,128)(2,1)} %constant_dynamic-update-slice_fusion), kind=kOutput, calls=%fused_computation.22 | convolution fusion | flops 2147483648 | bytes 8388608 | tf_op jit(solution)/shard_map/dot_general | solution.py:21
  165.5 0.0 reduce-scatter.3.cloned.1.call-update
  165.5 0.0 all-reduce.2.cloned.1.call-start
  165.5 272.1 %reduce-scatter.5.cloned.1.call-done = f32[128,4096]{0,1:T(8,128)} async-done(((f32[1024,4096]{0,1:T(8,128)}), f32[128,4096]{0,1:T(8,128)}) %reduce-scatter.5.cloned.1.call-update) | async-done | bytes 2097168 | tf_op jit(solution)/shard_map/reduce_scatter | solution.py:17
  437.6 0.0 all-reduce.2.cloned.1.call-update
  437.6 11.0 %reduce-scatter.3.cloned.1.call-done = f32[256,1024]{1,0:T(8,128)} async-done(((f32[512,1024]{1,0:T(8,128)}), f32[256,1024]{1,0:T(8,128)}) %reduce-scatter.3.cloned.1.call-update) | async-done | bytes 1048592 | tf_op jit(solution)/shard_map/reduce_scatter | solution.py:17
  448.6 2.1 convert_element_type.11
  450.7 64.3 %all-reduce.2.cloned.1.call-done = f32[128,4096]{0,1:T(8,128)} async-done(((f32[128,4096]{0,1:T(8,128)}), f32[128,4096]{0,1:T(8,128)}) %all-reduce.2.cloned.1.call-update) | async-done | bytes 2097168 | tf_op jit(solution)/shard_map/psum | solution.py:81
  515.0 2.4 multiply_reduce_fusion
  517.4 21.7 %psum.23 = f32[2048]{0:T(1024)S(1)} all-reduce(f32[2048]{0:T(1024)S(1)} %get-tuple-element.10), channel_id=1, replica_groups=mesh['rep'=2,'fs'=8,'tp'=2] {'fs'}, use_global_device_ids=true, to_apply=%region_6.7 | all-reduce | flops 2048 | bytes 16384 | tf_op jit(solution)/shard_map/psum | solution.py:86
  539.1 0.6 broadcast_multiply_fusion
  539.7 1.5 multiply_reduce_fusion.1
  541.2 2.5 psum.22
  543.7 0.5 broadcast_multiply_fusion.1
  544.2 1.3 copy.10
  (3 shorter events, 0.0 us)
Async XLA Ops:
  7.2 35.9 %copy-start.2 = (bf16[128,2048]{1,0:T(8,128)(2,1)S(1)}, bf16[128,2048]{1,0:T(8,128)(2,1)}, u32[]{:S(2)}) copy-start(bf16[128,2048]{1,0:T(8,128)(2,1)} %param.5) | copy-start | bytes 1572868
  7.2 111.5 %all-gather.4.cloned.1.call-start = ((), (), s32[]{:S(2)}) async-start(), calls=%async_computation.2 | async-start | bytes 1572864 | tf_op jit(solution)/shard_map/all_gather | solution.py:31
  7.9 117.6 %all-gather.6.cloned.1.call-start = ((), (), s32[]{:S(2)}) async-start(), calls=%async_computation.3 | async-start | bytes 1572864 | tf_op jit(solution)/shard_map/all_gather | solution.py:32
  8.7 132.2 %all-gather.8.cloned.1.call-start = ((), (), s32[]{:S(2)}) async-start(), calls=%async_computation.4 | async-start | bytes 4718592 | tf_op jit(solution)/shard_map/all_gather | solution.py:11
  9.4 428.2 %reduce-scatter.5.cloned.1.call-start = ((), (), s32[]{:S(2)}) async-start(), calls=%async_computation.6 | async-start | bytes 18874368 | tf_op jit(solution)/shard_map/reduce_scatter | solution.py:17
  9.4 25.8 %collective-permute-start = (bf16[128,2048]{1,0:T(8,128)(2,1)}, bf16[128,2048]{1,0:T(8,128)(2,1)S(1)}, u32[]{:S(2)}, u32[]{:S(2)}) collective-permute-start(bf16[128,2048]{1,0:T(8,128)(2,1)} %param.5), channel_id=1, source_target_pairs={{0,2},{2,4},{4,6},{6,8},{8,10},{10,12},{12,14},{14,0},{1,3},{3,5},... | collective-permute-start | bytes 1572872 | tf_op jit(solution)/shard_map/ppermute | solution.py:43
  12.5 25.1 %collective-permute-start.1 = (bf16[128,2048]{1,0:T(8,128)(2,1)}, bf16[128,2048]{1,0:T(8,128)(2,1)S(1)}, u32[]{:S(2)}, u32[]{:S(2)}) collective-permute-start(bf16[128,2048]{1,0:T(8,128)(2,1)} %param.5), channel_id=1, source_target_pairs={{0,14},{2,0},{4,2},{6,4},{8,6},{10,8},{12,10},{14,12},{1,15},{3,1}... | collective-permute-start | bytes 1572872 | tf_op jit(solution)/shard_map/ppermute | solution.py:46
  35.2 29.6 %collective-permute-start.2 = (bf16[128,2048]{1,0:T(8,128)(2,1)S(1)}, bf16[128,2048]{1,0:T(8,128)(2,1)S(1)}, u32[]{:S(2)}, u32[]{:S(2)}) collective-permute-start(bf16[128,2048]{1,0:T(8,128)(2,1)S(1)} %collective-permute-done), channel_id=1, source_target_pairs={{0,2},{2,4},{4,6},{6,8},{8,10},{10,12},{12,14},{14,0},{1,3},{3,5},... | collective-permute-start | bytes 1572872 | tf_op jit(solution)/shard_map/ppermute | solution.py:43
  37.6 31.3 %collective-permute-start.3 = (bf16[128,2048]{1,0:T(8,128)(2,1)S(1)}, bf16[128,2048]{1,0:T(8,128)(2,1)S(1)}, u32[]{:S(2)}, u32[]{:S(2)}) collective-permute-start(bf16[128,2048]{1,0:T(8,128)(2,1)S(1)} %collective-permute-done.1), channel_id=1, source_target_pairs={{0,14},{2,0},{4,2},{6,4},{8,6},{10,8},{12,10},{14,12},{1,15},{3,1}... | collective-permute-start | bytes 1572872 | tf_op jit(solution)/shard_map/ppermute | solution.py:46
  64.8 26.5 %collective-permute-start.4 = (bf16[128,2048]{1,0:T(8,128)(2,1)S(1)}, bf16[128,2048]{1,0:T(8,128)(2,1)S(1)}, u32[]{:S(2)}, u32[]{:S(2)}) collective-permute-start(bf16[128,2048]{1,0:T(8,128)(2,1)S(1)} %collective-permute-done.2), channel_id=1, source_target_pairs={{0,2},{2,4},{4,6},{6,8},{8,10},{10,12},{12,14},{14,0},{1,3},{3,5},... | collective-permute-start | bytes 1572872 | tf_op jit(solution)/shard_map/ppermute | solution.py:43
  68.9 24.1 %collective-permute-start.5 = (bf16[128,2048]{1,0:T(8,128)(2,1)S(1)}, bf16[128,2048]{1,0:T(8,128)(2,1)S(1)}, u32[]{:S(2)}, u32[]{:S(2)}) collective-permute-start(bf16[128,2048]{1,0:T(8,128)(2,1)S(1)} %collective-permute-done.3), channel_id=1, source_target_pairs={{0,14},{2,0},{4,2},{6,4},{8,6},{10,8},{12,10},{14,12},{1,15},{3,1}... | collective-permute-start | bytes 1572872 | tf_op jit(solution)/shard_map/ppermute | solution.py:46
  91.3 26.6 %collective-permute-start.6 = (bf16[128,2048]{1,0:T(8,128)(2,1)S(1)}, bf16[128,2048]{1,0:T(8,128)(2,1)S(1)}, u32[]{:S(2)}, u32[]{:S(2)}) collective-permute-start(bf16[128,2048]{1,0:T(8,128)(2,1)S(1)} %collective-permute-done.4), channel_id=1, source_target_pairs={{0,2},{2,4},{4,6},{6,8},{8,10},{10,12},{12,14},{14,0},{1,3},{3,5},... | collective-permute-start | bytes 1572872 | tf_op jit(solution)/shard_map/ppermute | solution.py:43
  125.5 15.4 %copy-start.1 = (bf16[512,1024]{1,0:T(8,128)(2,1)S(1)}, bf16[512,1024]{1,0:T(8,128)(2,1)}, u32[]{:S(2)}) copy-start(bf16[512,1024]{1,0:T(8,128)(2,1)} %all-gather.6.cloned.1.call-done) | copy-start | bytes 3145732
  133.7 14.5 %copy-start.3 = (bf16[512,1024]{1,0:T(8,128)(2,1)S(1)}, bf16[512,1024]{1,0:T(8,128)(2,1)}, u32[]{:S(2)}) copy-start(bf16[512,1024]{1,0:T(8,128)(2,1)} %all-gather.4.cloned.1.call-done) | copy-start | bytes 3145732
  146.9 1.3 copy-start.4
  148.2 3.4 copy-start
  158.0 1.6 copy-start.5
  158.0 290.6 %reduce-scatter.3.cloned.1.call-start = ((), (), s32[]{:S(2)}) async-start(), calls=%async_computation.5 | async-start | bytes 3145728 | tf_op jit(solution)/shard_map/reduce_scatter | solution.py:17
  165.5 349.6 %all-reduce.2.cloned.1.call-start = ((), (), s32[]{:S(2)}) async-start(), calls=%async_computation.7 | async-start | bytes 4194304 | tf_op jit(solution)/shard_map/psum | solution.py:81
Sparse Core Ops, SparseCore 0:
  9.5 11.7 all-gather.3
  22.9 10.1 all-gather.5
  35.1 105.7 all-gather.7
  158.1 279.4 reduce-scatter.4
  439.7 8.8 reduce-scatter.2
  450.8 64.2 all-reduce.1
